TPU v7x, 256 devices: a whole 4x4x8 slice. The times are simulated.
256 devices in a mesh: ep: 16 (over y, x), tp: 16 (over z, core).
Axes of the slice: x: 4, y: 4, z: 8, core: 2. Of those that a mesh axis runs over, the one named last changes fastest.
Arguments:
- query_latent: bfloat16 [8192, 1024], P('ep'), may hold values from -6 to 6
- joint_latent: bfloat16 [8192, 512], P('ep'), may hold values from -6 to 6
- rotary_key: bfloat16 [8192, 32], P('ep'), may hold values from -60 to 60
- query_gain: float32 [1024], replicated, may hold values from 0.1 to 1.9
- joint_gain: float32 [512], replicated, may hold values from 0.1 to 1.9
- query_weight: bfloat16 [1024, 2048], P(None, 'tp'), may hold values from -0.1875 to 0.1875
- query_rotary: bfloat16 [1024, 1024], P(None, 'tp'), may hold values from -0.1875 to 0.1875
- key_weight: bfloat16 [512, 2048], P(None, 'tp'), may hold values from -0.25 to 0.25
- value_weight: bfloat16 [512, 2048], P(None, 'tp'), may hold values from -0.25 to 0.25
- output_weight: bfloat16 [2048, 2048], P('tp'), may hold values from -6 to 6
- expert_input: bfloat16 [8192, 2048], P('ep'), may hold values from -6 to 6
- expert_gain: float32 [2048], replicated, may hold values from 0.1 to 1.9
- routes: int32 [8192, 2], P('ep'), may hold values from 0 to 31, all different within a row; in each aligned block of 512 rows (0 to 511, 512 to 1023, ...) at most 48 rows name the same one
- route_weight: float32 [8192, 2], P('ep'), may hold values from 0.2 to 1
- gate_weight: bfloat16 [32, 2048, 4096], P('ep', None, 'tp'), may hold values from -0.125 to 0.125
- up_weight: bfloat16 [32, 2048, 4096], P('ep', None, 'tp'), may hold values from -0.125 to 0.125
- down_weight: bfloat16 [32, 4096, 2048], P('ep', 'tp'), may hold values from -0.09375 to 0.09375
Outputs:
- mixer_out: bfloat16 [8192, 2048], P(('ep', 'tp'))
- expert_out: bfloat16 [8192, 2048], P('ep', 'tp')
Inputs may be any that keep to these rules, and one draw needn't show every extreme that they name: `routes`: A row names 2 different experts. Among the rows of one device (aligned blocks of 512 rows) no expert is named by more than 48 rows, a bound that some block reaches.
All inputs are finite; a program needn't handle non-finite values.
Results may differ from a plain program's by a relative error of at most 0.019.
The roundings to bfloat16 on the way count: a program that leaves them out, or rounds other values in their place, can miss the bound.
Values may be sent and summed in bfloat16 or wider, within the bound.
A program may use at most 128 MiB of HBM per device.

v0:
```python
import jax
import jax.numpy as jnp
from jax import lax
from jax.sharding import PartitionSpec as P

NOPE = 64
VDIM = 64
NORM_EPSILON = 1e-06
ROTARY_BASE = 10000.0


def sent_together(arrays, axis, dim, along):
    both = jnp.concatenate(arrays, axis=along)
    out, at, outs = (lax.all_gather(both, axis, axis=dim, tiled=True), 0, [])
    for a in arrays:
        outs.append(lax.slice_in_dim(out, at, at + a.shape[along], axis=along))
        at += a.shape[along]
    return tuple(outs)


def norm_rows(source, gain_vector):
    as_float = source.astype(jnp.float32)
    factor = lax.rsqrt(jnp.mean(as_float * as_float, axis=-1, keepdims=True) + NORM_EPSILON)
    return (as_float * factor * gain_vector).astype(jnp.bfloat16)


def rotate(source, positions):
    half_width = source.shape[-1] // 2
    frequencies = ROTARY_BASE ** (-jnp.arange(half_width, dtype=jnp.float32) / half_width)
    angles = positions[:, None] * frequencies[None, :]
    view_shape = (source.shape[0],) + (1,) * (source.ndim - 2) + (half_width,)
    cosine_table = jnp.cos(angles).reshape(view_shape)
    sine_table = jnp.sin(angles).reshape(view_shape)
    first_half = source[..., :half_width]
    second = source[..., half_width:]
    return jnp.concatenate(
        [
            first_half * cosine_table - second * sine_table,
            second * cosine_table + first_half * sine_table,
        ],
        axis=-1,
    )


def attend_block(
    carried, query_plain, query_turned, key_block, value_block, turned_block, score_scale
):
    row_top, row_total, mixed_values = carried
    scores = jnp.einsum("qhd,khd->qhk", query_plain, key_block, preferred_element_type=jnp.float32)
    scores = scores + jnp.einsum(
        "qhd,kd->qhk", query_turned, turned_block, preferred_element_type=jnp.float32
    )
    scores = scores * score_scale
    new_top = jnp.maximum(row_top, jnp.max(scores, axis=-1))
    factor = jnp.exp(row_top - new_top)
    expo = jnp.exp(scores - new_top[..., None])
    row_total = row_total * factor + jnp.sum(expo, axis=-1)
    mixed_values = mixed_values * factor[..., None] + jnp.einsum(
        "qhk,khd->qhd", expo.astype(jnp.bfloat16), value_block, preferred_element_type=jnp.float32
    )
    return (new_top, row_total, mixed_values)


def token_mixer(
    query_latent,
    joint_latent,
    rotary_key,
    query_gain,
    joint_gain,
    query_weight,
    query_rotary,
    key_weight,
    value_weight,
    output_weight,
):
    row_count = query_latent.shape[0]
    head_count = key_weight.shape[1] // NOPE
    turn_width = rotary_key.shape[1]
    offset = lax.axis_index("ep") * row_count
    positions = (offset + jnp.arange(row_count, dtype=jnp.int32)).astype(jnp.float32)
    query_normed = norm_rows(query_latent, query_gain)
    joint_normed = norm_rows(joint_latent, joint_gain)
    turned_key = rotate(rotary_key.astype(jnp.float32), positions).astype(jnp.bfloat16)
    query_plain = jnp.dot(query_normed, query_weight, preferred_element_type=jnp.float32).astype(
        jnp.bfloat16
    )
    query_plain = query_plain.reshape(row_count, head_count, NOPE)
    query_turned = jnp.dot(query_normed, query_rotary, preferred_element_type=jnp.float32)
    query_turned = rotate(
        query_turned.reshape(row_count, head_count, turn_width), positions
    ).astype(jnp.bfloat16)
    score_scale = (NOPE + turn_width) ** (-0.5)
    start_carry = (
        jnp.full((row_count, head_count), -jnp.inf, jnp.float32),
        jnp.zeros((row_count, head_count), jnp.float32),
        jnp.zeros((row_count, head_count, VDIM), jnp.float32),
    )
    carried = start_carry
    latent_piece, turned_piece = sent_together((joint_normed, turned_key), "ep", 0, 1)
    block_rows = min(row_count, latent_piece.shape[0])
    block_total = latent_piece.shape[0] // block_rows

    def scan_step(inner_carry, key_items):
        latent_block, turned_block = key_items
        key_block = jnp.dot(latent_block, key_weight, preferred_element_type=jnp.float32)
        key_block = key_block.astype(jnp.bfloat16).reshape(block_rows, head_count, NOPE)
        value_block = jnp.dot(latent_block, value_weight, preferred_element_type=jnp.float32)
        value_block = value_block.astype(jnp.bfloat16).reshape(block_rows, head_count, VDIM)
        return (
            attend_block(
                inner_carry,
                query_plain,
                query_turned,
                key_block,
                value_block,
                turned_block,
                score_scale,
            ),
            None,
        )

    carried, _ = lax.scan(
        scan_step,
        carried,
        (
            latent_piece.reshape(block_total, block_rows, latent_piece.shape[1]),
            turned_piece.reshape(block_total, block_rows, turn_width),
        ),
    )
    row_top, row_total, mixed_values = carried
    attended = (
        (mixed_values / row_total[..., None])
        .astype(jnp.bfloat16)
        .reshape(row_count, head_count * VDIM)
    )
    return lax.psum_scatter(
        jnp.dot(attended, output_weight, preferred_element_type=jnp.float32).astype(jnp.bfloat16),
        "tp",
        scatter_dimension=0,
        tiled=True,
    )


def experts(expert_input, expert_gain, routes, route_weight, gate_weight, up_weight, down_weight):
    row_count = expert_input.shape[0]
    feature_width = expert_input.shape[1]
    top_count = routes.shape[1]
    group_count = lax.axis_size("ep")
    local_count = gate_weight.shape[0]
    expert_count = local_count * group_count
    capacity = 3 * row_count // (2 * group_count)
    part_width = feature_width // lax.axis_size("tp")
    flat_routes = routes.reshape(-1)
    onehot = (flat_routes[:, None] == jnp.arange(expert_count, dtype=jnp.int32)[None, :]).astype(
        jnp.int32
    )
    rank_within = jnp.sum((jnp.cumsum(onehot, axis=0) - onehot) * onehot, axis=1)
    slot_index = flat_routes * capacity + rank_within
    owner_token = jnp.arange(row_count * top_count, dtype=jnp.int32) // top_count
    slot_token = jnp.zeros((expert_count * capacity,), jnp.int32).at[slot_index].set(owner_token)
    filled = jnp.zeros((expert_count * capacity,), jnp.bfloat16).at[slot_index].set(1.0)
    normed = norm_rows(expert_input, expert_gain)
    columns = lax.dynamic_slice_in_dim(normed, lax.axis_index("tp") * part_width, part_width, 1)
    outgoing = (columns[slot_token] * filled[:, None]).reshape(
        group_count, local_count, capacity, part_width
    )
    arrived = lax.all_to_all(outgoing, "ep", split_axis=0, concat_axis=0, tiled=True)
    piece = lax.all_gather(arrived, "tp", axis=3, tiled=True)
    gate_running = jnp.einsum(
        "secd,edf->secf", piece, gate_weight, preferred_element_type=jnp.float32
    )
    up_running = jnp.einsum("secd,edf->secf", piece, up_weight, preferred_element_type=jnp.float32)
    hidden = (jax.nn.silu(gate_running) * up_running).astype(jnp.bfloat16)
    partial_value = jnp.einsum(
        "secf,efd->secd", hidden, down_weight, preferred_element_type=jnp.float32
    )
    summed = lax.psum_scatter(
        partial_value.astype(jnp.bfloat16), "tp", scatter_dimension=3, tiled=True
    )
    returned = lax.all_to_all(summed, "ep", split_axis=0, concat_axis=0, tiled=True)
    picked = returned.reshape(expert_count * capacity, part_width)[slot_index]
    picked = picked.astype(jnp.float32).reshape(row_count, top_count, part_width)
    return jnp.sum(picked * route_weight[:, :, None], axis=1).astype(jnp.bfloat16)


def local(
    query_latent,
    joint_latent,
    rotary_key,
    query_gain,
    joint_gain,
    query_weight,
    query_rotary,
    key_weight,
    value_weight,
    output_weight,
    expert_input,
    expert_gain,
    routes,
    route_weight,
    gate_weight,
    up_weight,
    down_weight,
):
    mixer_out = token_mixer(
        query_latent,
        joint_latent,
        rotary_key,
        query_gain,
        joint_gain,
        query_weight,
        query_rotary,
        key_weight,
        value_weight,
        output_weight,
    )
    expert_out = experts(
        expert_input, expert_gain, routes, route_weight, gate_weight, up_weight, down_weight
    )
    return (mixer_out, expert_out)


def solution(mesh):
    return jax.shard_map(
        local,
        mesh=mesh,
        in_specs=(
            P("ep", None),
            P("ep", None),
            P("ep", None),
            P(),
            P(),
            P(None, "tp"),
            P(None, "tp"),
            P(None, "tp"),
            P(None, "tp"),
            P("tp", None),
            P("ep", None),
            P(),
            P("ep", None),
            P("ep", None),
            P("ep", None, "tp"),
            P("ep", None, "tp"),
            P("ep", "tp", None),
        ),
        out_specs=(P(("ep", "tp"), None), P("ep", "tp")),
        check_vma=False,
    )
```

profile of v0, /device:TPU:6, one launch (start us, length us, event | category | flops | bytes accessed | tf_op | source)
XLA Modules:
  0.0 353.4 jit_solution(10818710300028206992)
XLA Ops:
  7.2 4.2 %convert_element_type.83 = f32[512,2048]{1,0:T(8,128)} convert(bf16[512,2048]{1,0:T(8,128)(2,1)} %param.29) | non-fusion elementwise | flops 1048576 | bytes 6291456 | tf_op jit(solution)/shard_map/convert_element_type | solution.py:22
  12.7 9.0 %reduce-window.6 = s32[32,8,128]{2,1,0:T(8,128)S(1)} reduce-window(s32[32,8,128]{2,1,0:T(8,128)S(1)} %fusion.46, s32[]{:T(128)} %constant.30.clone.1), window={size=1x1x128 pad=0_0x0_0x127_0}, to_apply=%region_8.9 | reduce-window | flops 4161536 | bytes 262148 | tf_op jit(solution)/shard_map/reduce-window
  22.6 4.3 %scatter_custom_fusion = s32[1536]{0:T(1024)S(1)} fusion(s32[1024]{0:T(1024)S(1)} %bitcast.150, s32[1024]{0:T(1024)S(1)} %add_select_fusion, s32[]{:T(128)} %constant.30.clone.1), kind=kCustom, calls=%fused_computation.89 | custom fusion | bytes 6148 | tf_op jit(solution)/shard_map/scatter | solution.py:160
  26.9 7.6 %scatter_custom_fusion.1 = bf16[1536]{0:T(1024)(128)(2,1)S(1)} fusion(s32[1024]{0:T(1024)S(1)} %bitcast.151, bf16[1024]{0:T(1024)(128)(2,1)S(1)} %broadcast.163, bf16[]{:T(256)} %constant.82.clone.1), kind=kCustom, calls=%fused_computation.93 | custom fusion | bytes 3074 | tf_op jit(solution)/shard_map/scatter | solution.py:161
  36.5 3.2 gather_fusion
  40.0 14.7 %all_to_all.10 = bf16[16,2,48,128]{3,2,1,0:T(8,128)(2,1)S(1)} all-to-all(bf16[16,2,48,128]{3,2,1,0:T(8,128)(2,1)S(1)} %broadcast_multiply_fusion), channel_id=1, replica_groups=mesh['ep'=16,'tp'=16] {'ep'}, dimensions={0} | all-to-all | bytes 786432 | tf_op jit(solution)/shard_map/all_to_all | solution.py:167
  57.8 1.9 pad_maximum_fusion
  60.3 1.5 fusion.38
  62.5 51.3 %all-gather.5.cloned.1.call-done = bf16[16,2,48,2048]{3,2,0,1:T(8,128)(2,1)} async-done(((bf16[16,2,48,128]{3,2,0,1:T(8,128)(2,1)}), bf16[16,2,48,2048]{3,2,0,1:T(8,128)(2,1)}) %all-gather.5.cloned.1.call-update) | async-done | bytes 6291472 | tf_op jit(solution)/shard_map/all_gather | solution.py:168
  113.8 6.3 %fusion.23 = f32[2,16,48,256]{3,2,1,0:T(8,128)} fusion(bf16[16,2,48,2048]{3,2,0,1:T(8,128)(2,1)} %all-gather.5.cloned.1.call-done, bf16[2,2048,256]{2,1,0:T(8,128)(2,1)} %param.33), kind=kOutput, calls=%fused_computation.40 | convolution fusion | flops 1610612736 | bytes 9961472 | tf_op jit(solution)/shard_map/secd,edf->secf/dot_general | solution.py:169
  120.1 10.0 %convert_bitcast_fusion = bf16[16,2,48,2048]{3,2,0,1:T(8,128)(2,1)} fusion(bf16[2,256,2048]{2,1,0:T(8,128)(2,1)S(1)} %copy-done, f32[2,16,48,256]{3,2,1,0:T(8,128)} %fusion.23, bf16[16,2,48,2048]{3,2,0,1:T(8,128)(2,1)} %all-gather.5.cloned.1.call-done, bf16[2,2048,256]{2,1,0:T(8,128)(2,1)} %param.34), kind=kOutput, calls=%fused_computation.29 | convolution fusion | flops 3226730496 | bytes 18350080 | tf_op jit(solution)/shard_map/secf,efd->secd/dot_general | solution.py:174
  130.1 23.1 %copy.56 = bf16[16,2,48,2048]{2,0,1,3:T(8,128)(2,1)} copy(bf16[16,2,48,2048]{3,2,0,1:T(8,128)(2,1)} %convert_bitcast_fusion) | data formatting | bytes 12582912
  153.2 29.8 %reshape.224 = bf16[2048,1536]{1,0:T(8,128)(2,1)} reshape(bf16[2048,2,16,48]{3,2,1,0:T(8,128)(2,1)} %bitcast.135) | data formatting | bytes 12582912
  183.3 17.5 %all-gather.3.cloned.1.call-done = bf16[8192,544]{1,0:T(8,128)(2,1)} async-done(((bf16[512,544]{1,0:T(8,128)(2,1)}), bf16[8192,544]{1,0:T(8,128)(2,1)}) %all-gather.3.cloned.1.call-update) | async-done | bytes 8912912 | tf_op jit(solution)/shard_map/all_gather | solution.py:14
  200.8 1.6 slice-done
  203.2 7.2 %slice.38 = bf16[8192,512]{1,0:T(8,128)(2,1)} slice(bf16[8192,544]{1,0:T(8,128)(2,1)} %all-gather.3.cloned.1.call-done), slice={[0:8192], [0:512]} | slice | bytes 16777216 | tf_op jit(solution)/shard_map/slice | solution.py:16
  210.4 73.0 %while.15 = (s32[]{:T(128)}, f32[512,2]{0,1:T(2,128)S(1)}, f32[512,2]{0,1:T(2,128)S(1)}, f32[512,2,64]{0,2,1:T(8,128)S(1)}, bf16[16,512,512]{2,1,0:T(8,128)(2,1)...) while((s32[]{:T(128)}, f32[512,2]{0,1:T(2,128)S(1)}, ...), condition=%wide.region_5.6_spmd.clone, body=%wide.region_2.5_spmd.clone.sunk | while | flops 305992704 | bytes 13141125 | solution.py:122
  213.1 1.4 convolution_convert_fusion.7
  215.0 1.4 convolution_convert_fusion.6
  219.5 1.4 convolution_convert_fusion.6
  222.2 1.4 convolution_convert_fusion.7
  226.8 1.4 convolution_convert_fusion.7
  228.7 1.4 convolution_convert_fusion.6
  233.2 1.4 convolution_convert_fusion.6
  235.9 1.4 convolution_convert_fusion.7
  240.5 1.4 convolution_convert_fusion.7
  242.4 1.4 convolution_convert_fusion.6
  245.1 1.4 convolution_convert_fusion.7
  247.0 1.4 convolution_convert_fusion.6
  249.6 1.4 convolution_convert_fusion.7
  251.5 1.4 convolution_convert_fusion.6
  254.2 1.4 convolution_convert_fusion.7
  256.1 1.4 convolution_convert_fusion.6
  258.8 1.4 convolution_convert_fusion.7
  263.3 1.4 convolution_convert_fusion.7
  267.9 1.4 convolution_convert_fusion.7
  269.8 1.4 convolution_convert_fusion.6
  272.5 1.4 convolution_convert_fusion.7
  277.0 1.4 convolution_convert_fusion.7
  281.6 1.4 convolution_convert_fusion.7
  283.5 3.1 convolution_convert_fusion.2
  286.7 2.1 reshape.225
  288.8 1.8 copy.48
  290.6 5.7 %all-to-all-start.1 = ((bf16[16,2,48,128]{3,2,1,0:T(8,128)(2,1)}), bf16[16,2,48,128]{3,2,1,0:T(8,128)(2,1)S(1)}, u32[]{:S(2)}, u32[]{:S(2)}) async-start(bf16[16,2,48,128]{3,2,1,0:T(8,128)(2,1)} %copy.48), calls=%async_computation.2 | async-start | bytes 786432 | tf_op jit(solution)/shard_map/all_to_all | solution.py:180
  296.5 7.1 %all-to-all-done.1 = bf16[16,2,48,128]{3,2,1,0:T(8,128)(2,1)S(1)} async-done(((bf16[16,2,48,128]{3,2,1,0:T(8,128)(2,1)}), bf16[16,2,48,128]{3,2,1,0:T(8,128)(2,1)S(1)}, u32[]{:S(2)}, u32[]{:S(2)}) %all-to-all-start.1) | async-done | bytes 393248 | tf_op jit(solution)/shard_map/all_to_all | solution.py:180
  303.6 3.2 gather_fusion.1
  306.8 3.5 fusion.37
  310.3 36.6 %reduce-scatter.5.cloned.1.call-done = bf16[32,2048]{1,0:T(8,128)(2,1)} async-done(((bf16[512,2048]{1,0:T(8,128)(2,1)}), bf16[32,2048]{1,0:T(8,128)(2,1)}) %reduce-scatter.5.cloned.1.call-update) | async-done | bytes 131088 | tf_op jit(solution)/shard_map/reduce_scatter | solution.py:136
  (210 shorter events, 50.3 us)
Async XLA Ops:
  7.2 113.0 %copy-start = (bf16[2,256,2048]{2,1,0:T(8,128)(2,1)S(1)}, bf16[2,256,2048]{2,1,0:T(8,128)(2,1)}, u32[]{:S(2)}) copy-start(bf16[2,256,2048]{2,1,0:T(8,128)(2,1)} %param.35) | copy-start | bytes 6291460
  7.2 106.6 %all-gather.5.cloned.1.call-start = ((), (), s32[]{:S(2)}) async-start(), calls=%async_computation.6 | async-start | bytes 6684672 | tf_op jit(solution)/shard_map/all_gather | solution.py:168
  7.2 4.2 %copy-start.2 = (bf16[512,2048]{1,0:T(8,128)(2,1)S(1)}, bf16[512,2048]{1,0:T(8,128)(2,1)}, u32[]{:S(2)}) copy-start(bf16[512,2048]{1,0:T(8,128)(2,1)} %param.29) | copy-start | bytes 6291460
  11.4 0.7 copy-start.11
  39.7 15.9 %copy-start.10 = (bf16[512,32]{0,1:T(8,128)(2,1)S(1)}, bf16[512,32]{0,1:T(8,128)(2,1)}, u32[]{:S(2)}) copy-start(bf16[512,32]{0,1:T(8,128)(2,1)} %param.21) | copy-start | bytes 98308
  39.7 17.7 %copy-start.5 = (bf16[512,512]{1,0:T(8,128)(2,1)S(1)}, bf16[512,512]{1,0:T(8,128)(2,1)}, u32[]{:S(2)}) copy-start(bf16[512,512]{1,0:T(8,128)(2,1)} %param.20) | copy-start | bytes 1572868
  39.7 17.9 %copy-start.13 = (f32[512]{0:T(512)S(1)}, f32[512]{0:T(512)}, u32[]{:S(2)}) copy-start(f32[512]{0:T(512)} %param.23) | copy-start | bytes 6148
  55.5 145.3 %all-gather.3.cloned.1.call-start = ((), (), s32[]{:S(2)}) async-start(), calls=%async_computation.4 | async-start | bytes 11141120 | tf_op jit(solution)/shard_map/all_gather | solution.py:14
  57.6 2.8 copy-start.15
  57.8 2.3 copy-start.6
  59.7 2.1 copy-start.8
  59.7 2.1 copy-start.9
  59.8 226.9 %reduce-scatter.7.cloned.1.call-start = ((), (), s32[]{:S(2)}) async-start(), calls=%async_computation.7 | async-start | bytes 6684672
  60.0 1.9 copy-start.7
  60.0 1.9 copy-start.14
  183.0 163.8 %reduce-scatter.5.cloned.1.call-start = ((), (), s32[]{:S(2)}) async-start(), calls=%async_computation.5 | async-start | bytes 2228224 | tf_op jit(solution)/shard_map/reduce_scatter | solution.py:136
  200.8 1.6 slice-start
  203.2 7.2 %copy-start.3 = (bf16[512,128]{1,0:T(8,128)(2,1)S(1)}, bf16[512,128]{1,0:T(8,128)(2,1)}, u32[]{:S(2)}) copy-start(bf16[512,128]{1,0:T(8,128)(2,1)} %param.26) | copy-start | bytes 393220
  203.2 7.2 %copy-start.4 = (bf16[512,128]{1,0:T(8,128)(2,1)S(1)}, bf16[512,128]{1,0:T(8,128)(2,1)}, u32[]{:S(2)}) copy-start(bf16[512,128]{1,0:T(8,128)(2,1)} %param.27) | copy-start | bytes 393220
  286.6 9.6 %copy-start.12 = (f32[512,2]{0,1:T(2,128)S(1)}, f32[512,2]{0,1:T(2,128)}, u32[]{:S(2)}) copy-start(f32[512,2]{0,1:T(2,128)} %param.32) | copy-start | bytes 12292
  288.8 58.1 %copy-start.1 = (bf16[2,256,2048]{2,1,0:T(8,128)(2,1)S(1)}, bf16[2,256,2048]{2,1,0:T(8,128)(2,1)}, u32[]{:S(2)}) copy-start(bf16[2,256,2048]{2,1,0:T(8,128)(2,1)} %param.35) | copy-start | bytes 6291460
  290.6 13.0 %all-to-all-start.1 = ((bf16[16,2,48,128]{3,2,1,0:T(8,128)(2,1)}), bf16[16,2,48,128]{3,2,1,0:T(8,128)(2,1)S(1)}, u32[]{:S(2)}, u32[]{:S(2)}) async-start(bf16[16,2,48,128]{3,2,1,0:T(8,128)(2,1)} %copy.48), calls=%async_computation.2 | async-start | bytes 786432 | tf_op jit(solution)/shard_map/all_to_all | solution.py:180
Sparse Core Ops, SparseCore 0:
  55.7 58.0 all-gather.4
  116.2 84.5 all-gather.2
  203.4 66.9 reduce-scatter.6
  286.8 60.0 reduce-scatter.4
where the time goes:
time: 356 us; the launch traced here: 353 us
  waiting for transfers between devices  113 us (32%)
  local copies, waits for them, and re-layouts  88.8 us (25%)
  matrix products  88.1 us (25%)
  other arithmetic  27.5 us (8%)
  blocking collectives  14.7 us (4%)
  between operations  14.3 us (4%)
  starting transfers between devices  6.26 us (2%)
    unnamed x38, local copies, waits for them, and re-layouts  56.3 us
    all_gather x1, waiting for transfers between devices, experts(): piece = lax.all_gather(arrived, 'tp', axis=3, tiled=True)  51.3 us
    reduce_scatter x1, waiting for transfers between devices, token_mixer(): lax.psum_scatter(jnp.dot(attended, output_weight, preferred_element_type=...  36.6 us
    dot_general x16, matrix products, scan_step(): jnp.dot(latent_block, value_weight, preferred_element_type=jnp.float32)  21.8 us
    dot_general x16, matrix products, scan_step(): jnp.dot(latent_block, key_weight, preferred_element_type=jnp.float32)  21.7 us
    all_gather x1, waiting for transfers between devices, sent_together(): out, at, outs = (lax.all_gather(both, axis, axis=dim, tiled=True), 0, [])  17.5 us
    all_to_all x1, blocking collectives, experts(): lax.all_to_all(outgoing, 'ep', split_axis=0, concat_axis=0, tiled=True)  14.7 us
    dot_general x1, matrix products, experts(): jnp.einsum('secf,efd->secd', hidden, down_weight, preferred_element_type=...  10 us
  transfers between devices with their start and end apart: 5, of which 4 were waited for; matrix products, arithmetic and copies ran while one was open for 48% of the time, Pallas kernels for 0%

commit v1 on v0

--- a/solution.py
+++ b/solution.py
@@ -165,7 +165,10 @@
         group_count, local_count, capacity, part_width
     )
     arrived = lax.all_to_all(outgoing, "ep", split_axis=0, concat_axis=0, tiled=True)
-    piece = lax.all_gather(arrived, "tp", axis=3, tiled=True)
+    peers = lax.axis_size("tp")
+    blocks = jnp.stack([arrived for _ in range(peers)])
+    blocks = lax.all_to_all(blocks, "tp", split_axis=0, concat_axis=0)
+    piece = jnp.concatenate(blocks, axis=3)
     gate_running = jnp.einsum(
         "secd,edf->secf", piece, gate_weight, preferred_element_type=jnp.float32
     )

time: 356 us -> 441 us (1.24)
  waiting for transfers between devices: 113 us -> 177 us
  starting transfers between devices: 6.26 us -> 17.6 us
    all_to_all x0 -> x1, waiting for transfers between devices: none -> 137 us  [experts(): blocks = lax.all_to_all(blocks, 'tp', split_axis=0, concat_axis=0)]
    all_gather x1 -> x0, waiting for transfers between devices: 51.3 us -> none  [experts(): piece = lax.all_gather(arrived, 'tp', axis=3, tiled=True)]
    all_gather x1, waiting for transfers between devices: 17.5 us -> 0.02 us  [sent_together(): out, at, outs = (lax.all_gather(both, axis, axis=dim, tiled=True), 0, [])]
    all_to_all x0 -> x1, starting transfers between devices: none -> 9.72 us  [experts(): blocks = lax.all_to_all(blocks, 'tp', split_axis=0, concat_axis=0)]
    unnamed x38 -> x26, local copies, waits for them, and re-layouts: 56.3 us -> 56 us
  transfers between devices with their start and end apart: 5 -> 5, of which waited for: 4 -> 3; matrix products, arithmetic and copies ran while one was open for 48% -> 46% of each run, Pallas kernels for 0% -> 0%
where the time goes in v1:
time: 441 us; the launch traced here: 438 us
  waiting for transfers between devices  177 us (40%)
  local copies, waits for them, and re-layouts  91.1 us (21%)
  matrix products  88 us (20%)
  other arithmetic  30.3 us (7%)
  starting transfers between devices  17.6 us (4%)
  blocking collectives  17.4 us (4%)
  between operations  15.9 us (4%)
    all_to_all x1, waiting for transfers between devices, experts(): blocks = lax.all_to_all(blocks, 'tp', split_axis=0, concat_axis=0)  137 us
    unnamed x26, local copies, waits for them, and re-layouts  56 us
    reduce_scatter x1, waiting for transfers between devices, token_mixer(): lax.psum_scatter(jnp.dot(attended, output_weight, preferred_element_type=...  33.1 us
    dot_general x16, matrix products, scan_step(): jnp.dot(latent_block, value_weight, preferred_element_type=jnp.float32)  21.7 us
    dot_general x16, matrix products, scan_step(): jnp.dot(latent_block, key_weight, preferred_element_type=jnp.float32)  21.7 us
    all_to_all x1, blocking collectives, experts(): lax.all_to_all(outgoing, 'ep', split_axis=0, concat_axis=0, tiled=True)  17.4 us
    dot_general x1, matrix products, experts(): jnp.einsum('secf,efd->secd', hidden, down_weight, preferred_element_type=...  9.94 us
    all_to_all x1, starting transfers between devices, experts(): blocks = lax.all_to_all(blocks, 'tp', split_axis=0, concat_axis=0)  9.72 us
  transfers between devices with their start and end apart: 5, of which 3 were waited for; matrix products, arithmetic and copies ran while one was open for 46% of the time, Pallas kernels for 0%

profile of v1, /device:TPU:6, one launch (start us, length us, event | category | flops | bytes accessed | tf_op | source)
XLA Modules:
  0.0 438.4 jit_solution(12087460164382789880)
XLA Ops:
  13.4 4.0 convert_element_type.83
  17.5 9.0 %reduce-window.6 = s32[32,8,128]{2,1,0:T(8,128)S(1)} reduce-window(s32[32,8,128]{2,1,0:T(8,128)S(1)} %fusion.54, s32[]{:T(128)} %constant.30.clone.1), window={size=1x1x128 pad=0_0x0_0x127_0}, to_apply=%region_8.9 | reduce-window | flops 4161536 | bytes 262148 | tf_op jit(solution)/shard_map/reduce-window
  27.4 4.3 scatter_custom_fusion
  31.7 7.6 %scatter_custom_fusion.1 = bf16[1536]{0:T(1024)(128)(2,1)S(1)} fusion(s32[1024]{0:T(1024)S(1)} %bitcast.167, bf16[1024]{0:T(1024)(128)(2,1)S(1)} %broadcast.165, bf16[]{:T(256)} %constant.82.clone.1), kind=kCustom, calls=%fused_computation.97 | custom fusion | bytes 3074 | tf_op jit(solution)/shard_map/scatter | solution.py:161
  40.2 2.1 multiply_reduce_fusion
  43.4 3.2 gather_fusion
  46.9 17.4 %all_to_all.15 = bf16[16,2,48,128]{3,2,1,0:T(8,128)(2,1)S(1)} all-to-all(bf16[16,2,48,128]{3,2,1,0:T(8,128)(2,1)S(1)} %broadcast_multiply_fusion), channel_id=1, replica_groups=mesh['ep'=16,'tp'=16] {'ep'}, dimensions={0} | all-to-all | bytes 786432 | tf_op jit(solution)/shard_map/all_to_all | solution.py:167
  64.3 4.1 stack.2
  68.4 9.7 %all-to-all-start.1 = ((bf16[16,16,2,48,128]{4,3,1,2,0:T(8,128)(2,1)}), bf16[16,16,2,48,128]{4,3,1,2,0:T(8,128)(2,1)}, u32[]{:S(2)}, u32[]{:S(2)}) async-start(bf16[16,16,2,48,128]{4,3,1,2,0:T(8,128)(2,1)} %stack.2), calls=%async_computation.2 | async-start | bytes 12582912 | tf_op jit(solution)/shard_map/all_to_all | solution.py:170
  78.7 1.5 fusion.46
  80.8 136.6 %all-to-all-done.1 = bf16[16,16,2,48,128]{4,3,1,2,0:T(8,128)(2,1)} async-done(((bf16[16,16,2,48,128]{4,3,1,2,0:T(8,128)(2,1)}), bf16[16,16,2,48,128]{4,3,1,2,0:T(8,128)(2,1)}, u32[]{:S(2)}, u32[]{:S(2)}) %all-to-all-start.1) | async-done | bytes 6291488 | tf_op jit(solution)/shard_map/all_to_all | solution.py:170
  217.4 6.3 %fusion.19 = f32[2,16,48,256]{3,2,1,0:T(8,128)} fusion(bf16[2,2048,256]{2,1,0:T(8,128)(2,1)} %param.33, bf16[16,16,2,48,128]{4,3,1,2,0:T(8,128)(2,1)} %all-to-all-done.1), kind=kOutput, calls=%fused_computation.31 | convolution fusion | flops 1610612736 | bytes 9961472 | tf_op jit(solution)/shard_map/secd,edf->secf/dot_general | solution.py:172
  223.7 9.9 %convert_bitcast_fusion = bf16[16,2,48,2048]{3,2,0,1:T(8,128)(2,1)} fusion(bf16[2,256,2048]{2,1,0:T(8,128)(2,1)S(1)} %copy-done, f32[2,16,48,256]{3,2,1,0:T(8,128)} %fusion.19, bf16[2,2048,256]{2,1,0:T(8,128)(2,1)} %param.34, bf16[16,16,2,48,128]{4,3,1,2,0:T(8,128)(2,1)} %all-to-all-done.1), kind=kOutput, calls=%fused_computation.33 | convolution fusion | flops 3226730496 | bytes 18350080 | tf_op jit(solution)/shard_map/secf,efd->secd/dot_general | solution.py:177
  233.7 23.1 %copy.57 = bf16[16,2,48,2048]{2,0,1,3:T(8,128)(2,1)} copy(bf16[16,2,48,2048]{3,2,0,1:T(8,128)(2,1)} %convert_bitcast_fusion) | data formatting | bytes 12582912
  256.7 29.7 %reshape.234 = bf16[2048,1536]{1,0:T(8,128)(2,1)} reshape(bf16[2048,2,16,48]{3,2,1,0:T(8,128)(2,1)} %bitcast.151) | data formatting | bytes 12582912
  286.7 1.6 slice-done
  289.1 7.2 %slice.38 = bf16[8192,512]{1,0:T(8,128)(2,1)} slice(bf16[8192,544]{1,0:T(8,128)(2,1)} %all-gather.2.cloned.1.call-done), slice={[0:8192], [0:512]} | slice | bytes 16777216 | tf_op jit(solution)/shard_map/slice | solution.py:16
  296.3 73.0 %while.15 = (s32[]{:T(128)}, f32[512,2]{0,1:T(2,128)S(1)}, f32[512,2]{0,1:T(2,128)S(1)}, f32[512,2,64]{0,2,1:T(8,128)S(1)}, bf16[16,512,512]{2,1,0:T(8,128)(2,1)...) while((s32[]{:T(128)}, f32[512,2]{0,1:T(2,128)S(1)}, ...), condition=%wide.region_5.6_spmd.clone, body=%wide.region_2.5_spmd.clone.sunk | while | flops 305992704 | bytes 13141125 | solution.py:122
  296.3 1.4 convolution_convert_fusion.6
  300.9 1.4 convolution_convert_fusion.6
  303.6 1.4 convolution_convert_fusion.7
  308.1 1.4 convolution_convert_fusion.7
  310.0 1.4 convolution_convert_fusion.6
  312.7 1.4 convolution_convert_fusion.7
  314.6 1.4 convolution_convert_fusion.6
  317.3 1.4 convolution_convert_fusion.7
  319.1 1.4 convolution_convert_fusion.6
  321.8 1.4 convolution_convert_fusion.7
  323.7 1.4 convolution_convert_fusion.6
  326.4 1.4 convolution_convert_fusion.7
  331.0 1.4 convolution_convert_fusion.7
  332.8 1.4 convolution_convert_fusion.6
  335.5 1.4 convolution_convert_fusion.7
  337.4 1.4 convolution_convert_fusion.6
  340.1 1.4 convolution_convert_fusion.7
  344.7 1.4 convolution_convert_fusion.7
  346.5 1.4 convolution_convert_fusion.6
  351.1 1.4 convolution_convert_fusion.6
  358.3 1.4 convolution_convert_fusion.7
  367.4 1.4 convolution_convert_fusion.7
  369.3 3.1 convolution_convert_fusion.2
  372.5 2.1 reshape.235
  374.7 1.8 copy.49
  376.5 7.3 %all-to-all-start.2 = ((bf16[16,2,48,128]{3,2,1,0:T(8,128)(2,1)}), bf16[16,2,48,128]{3,2,1,0:T(8,128)(2,1)S(1)}, u32[]{:S(2)}, u32[]{:S(2)}) async-start(bf16[16,2,48,128]{3,2,1,0:T(8,128)(2,1)} %copy.49), calls=%async_computation.3 | async-start | bytes 786432 | tf_op jit(solution)/shard_map/all_to_all | solution.py:183
  383.9 7.3 %all-to-all-done.2 = bf16[16,2,48,128]{3,2,1,0:T(8,128)(2,1)S(1)} async-done(((bf16[16,2,48,128]{3,2,1,0:T(8,128)(2,1)}), bf16[16,2,48,128]{3,2,1,0:T(8,128)(2,1)S(1)}, u32[]{:S(2)}, u32[]{:S(2)}) %all-to-all-start.2) | async-done | bytes 393248 | tf_op jit(solution)/shard_map/all_to_all | solution.py:183
  391.3 3.2 gather_fusion.1
  394.5 3.5 fusion.45
  397.9 33.1 %reduce-scatter.5.cloned.1.call-done = bf16[32,2048]{1,0:T(8,128)(2,1)} async-done(((bf16[512,2048]{1,0:T(8,128)(2,1)}), bf16[32,2048]{1,0:T(8,128)(2,1)}) %reduce-scatter.5.cloned.1.call-update) | async-done | bytes 131088 | tf_op jit(solution)/shard_map/reduce_scatter | solution.py:136
  (198 shorter events, 52.8 us)
Async XLA Ops:
  8.0 215.7 %copy-start = (bf16[2,256,2048]{2,1,0:T(8,128)(2,1)S(1)}, bf16[2,256,2048]{2,1,0:T(8,128)(2,1)}, u32[]{:S(2)}) copy-start(bf16[2,256,2048]{2,1,0:T(8,128)(2,1)} %param.35) | copy-start | bytes 6291460
  8.0 278.7 %all-gather.2.cloned.1.call-start = ((), (), s32[]{:S(2)}) async-start(), calls=%async_computation.5 | async-start | bytes 11141120 | tf_op jit(solution)/shard_map/all_gather | solution.py:14
  9.0 3.9 copy-start.6
  68.3 10.0 %copy-start.4 = (bf16[512,1024]{1,0:T(8,128)(2,1)S(1)}, bf16[512,1024]{1,0:T(8,128)(2,1)}, u32[]{:S(2)}) copy-start(bf16[512,1024]{1,0:T(8,128)(2,1)} %param.19) | copy-start | bytes 3145732
  68.4 10.3 %copy-start.9 = (f32[1024]{0:T(1024)S(1)}, f32[1024]{0:T(1024)}, u32[]{:S(2)}) copy-start(f32[1024]{0:T(1024)} %param.22) | copy-start | bytes 12292
  68.4 149.0 %all-to-all-start.1 = ((bf16[16,16,2,48,128]{4,3,1,2,0:T(8,128)(2,1)}), bf16[16,16,2,48,128]{4,3,1,2,0:T(8,128)(2,1)}, u32[]{:S(2)}, u32[]{:S(2)}) async-start(bf16[16,16,2,48,128]{4,3,1,2,0:T(8,128)(2,1)} %stack.2), calls=%async_computation.2 | async-start | bytes 12582912 | tf_op jit(solution)/shard_map/all_to_all | solution.py:170
  78.1 294.4 %reduce-scatter.7.cloned.1.call-start = ((), (), s32[]{:S(2)}) async-start(), calls=%async_computation.7 | async-start | bytes 6684672
  78.4 1.9 copy-start.5
  78.4 1.8 copy-start.8
  286.4 144.6 %reduce-scatter.5.cloned.1.call-start = ((), (), s32[]{:S(2)}) async-start(), calls=%async_computation.6 | async-start | bytes 2228224 | tf_op jit(solution)/shard_map/reduce_scatter | solution.py:136
  286.7 1.6 slice-start
  289.1 7.2 %copy-start.2 = (bf16[512,128]{1,0:T(8,128)(2,1)S(1)}, bf16[512,128]{1,0:T(8,128)(2,1)}, u32[]{:S(2)}) copy-start(bf16[512,128]{1,0:T(8,128)(2,1)} %param.26) | copy-start | bytes 393220
  289.1 7.2 %copy-start.3 = (bf16[512,128]{1,0:T(8,128)(2,1)S(1)}, bf16[512,128]{1,0:T(8,128)(2,1)}, u32[]{:S(2)}) copy-start(bf16[512,128]{1,0:T(8,128)(2,1)} %param.27) | copy-start | bytes 393220
  372.5 11.3 %copy-start.7 = (f32[512,2]{0,1:T(2,128)S(1)}, f32[512,2]{0,1:T(2,128)}, u32[]{:S(2)}) copy-start(f32[512,2]{0,1:T(2,128)} %param.32) | copy-start | bytes 12292
  374.6 56.3 %copy-start.1 = (bf16[2,256,2048]{2,1,0:T(8,128)(2,1)S(1)}, bf16[2,256,2048]{2,1,0:T(8,128)(2,1)}, u32[]{:S(2)}) copy-start(bf16[2,256,2048]{2,1,0:T(8,128)(2,1)} %param.35) | copy-start | bytes 6291460
  376.5 14.8 %all-to-all-start.2 = ((bf16[16,2,48,128]{3,2,1,0:T(8,128)(2,1)}), bf16[16,2,48,128]{3,2,1,0:T(8,128)(2,1)S(1)}, u32[]{:S(2)}, u32[]{:S(2)}) async-start(bf16[16,2,48,128]{3,2,1,0:T(8,128)(2,1)} %copy.49), calls=%async_computation.3 | async-start | bytes 786432 | tf_op jit(solution)/shard_map/all_to_all | solution.py:183
Sparse Core Ops, SparseCore 0:
  13.0 91.0 all-gather.1
Sparse Core Ops, SparseCore 1:
  286.5 65.5 reduce-scatter.6
  372.6 58.3 reduce-scatter.4
